TPU v7x, 32 devices: a whole 2x2x4 slice. The times are simulated.
32 devices in a mesh: sp: 8 (over z, y), tp: 4 (over x, core).
Axes of the slice: x: 2, y: 2, z: 4, core: 2. Of those that a mesh axis runs over, the one named last changes fastest.
Arguments:
- tokens: bfloat16 [1024, 2048], P(('sp', 'tp')), may hold values from -6 to 6
- doc_lengths: int32 [16], replicated, may hold values from 1 to 640, 1024 in all
- query_down: bfloat16 [2048, 512], replicated, may hold values from -0.125 to 0.125
- latent_down: bfloat16 [2048, 256], replicated, may hold values from -0.125 to 0.125
- rope_down: bfloat16 [2048, 32], replicated, may hold values from -0.125 to 0.125
- query_latent_gain: float32 [512], replicated, may hold values from 0.1 to 1.9
- latent_gain: float32 [256], replicated, may hold values from 0.1 to 1.9
- query_up: bfloat16 [512, 768], P(None, 'tp'), may hold values from -0.25 to 0.25
- key_up: bfloat16 [256, 512], P(None, 'tp'), may hold values from -0.375 to 0.375
- value_up: bfloat16 [256, 512], P(None, 'tp'), may hold values from -0.375 to 0.375
- query_gain: float32 [96], replicated, may hold values from 0.5 to 15
- key_gain: float32 [96], replicated, may hold values from 0.5 to 15
- output_gain: float32 [512], replicated, may hold values from 0.1 to 1.9
- output_weight: bfloat16 [512, 2048], P(None, 'tp'), may hold values from -0.25 to 0.25
Outputs:
- layer_output: bfloat16 [1024, 2048], P('sp', 'tp')
- log_totals: float32 [8, 1024], P('tp', 'sp')
Inputs may be any that keep to these rules, and one draw needn't show every extreme that they name: `doc_lengths`: the lengths sum to 1024; the longest is exactly 640.
All inputs are finite; a program needn't handle non-finite values.
Results may differ from a plain program's by a relative error of at most 0.019.
The roundings to bfloat16 on the way count: a program that leaves them out, or rounds other values in their place, can miss the bound.
Values may be sent and summed in bfloat16 or wider, within the bound.
A program may use at most 64 MiB of HBM per device.

v0:
```python
import math
import jax
import jax.numpy as jnp
from jax import lax
from jax.sharding import PartitionSpec as P

NOPE = 64
ROPE = 32
VD = 64
EPS = 1e-06
THETA = 10000.0
NEG = -1e30
key_span = 2048


def norm_rows(matrix, scaling):
    mean_square = jnp.mean(matrix * matrix, axis=-1, keepdims=True)
    return matrix * lax.rsqrt(mean_square + EPS) * scaling


def rotate(matrix, places):
    half_width = matrix.shape[-1] // 2
    inverse = THETA ** (-jnp.arange(half_width, dtype=jnp.float32) / half_width)
    angles = places.astype(jnp.float32)[:, None, None] * inverse
    cosine = jnp.cos(angles)
    sine_part = jnp.sin(angles)
    leading = matrix[..., :half_width]
    trailing = matrix[..., half_width:]
    return jnp.concatenate(
        [leading * cosine - trailing * sine_part, trailing * cosine + leading * sine_part], axis=-1
    )


def doc_index(places, doc_ends):
    return jnp.sum((places[:, None] >= doc_ends[None, :]).astype(jnp.int32), axis=1)


def head_keys(latent_rows, rope_rows, places, key_up, value_up, key_gain):
    row_count = latent_rows.shape[0]
    head_count = key_up.shape[1] // NOPE
    plain_part = jnp.dot(latent_rows, key_up, preferred_element_type=jnp.float32).reshape(
        row_count, head_count, NOPE
    )
    shared_part = jnp.broadcast_to(
        rope_rows.astype(jnp.float32)[:, None, :], (row_count, head_count, ROPE)
    )
    joined = norm_rows(jnp.concatenate([plain_part, shared_part], axis=-1), key_gain)
    key_block = jnp.concatenate(
        [joined[..., :NOPE], rotate(joined[..., NOPE:], places)], axis=-1
    ).astype(jnp.bfloat16)
    value_block = jnp.dot(latent_rows, value_up, preferred_element_type=jnp.float32).astype(
        jnp.bfloat16
    )
    return (key_block, value_block.reshape(row_count, head_count, VD))


def absorb_block(running, queries, query_docs, key_block, value_block, key_docs, score_scale):
    row_top, row_total, weighted = running
    scores = (
        jnp.einsum("qhd,khd->hqk", queries, key_block, preferred_element_type=jnp.float32)
        * score_scale
    )
    allowed = (query_docs[:, None] == key_docs[None, :])[None]
    scores = jnp.where(allowed, scores, NEG)
    newest_top = jnp.maximum(row_top, jnp.max(scores, axis=-1))
    weights = jnp.where(allowed, jnp.exp(scores - newest_top[..., None]), 0.0)
    rescale = jnp.exp(row_top - newest_top)
    row_total = row_total * rescale + jnp.sum(weights, axis=-1)
    update = jnp.einsum(
        "hqk,khd->qhd",
        weights.astype(jnp.bfloat16),
        value_block,
        preferred_element_type=jnp.float32,
    )
    weighted = weighted * jnp.transpose(rescale)[:, :, None] + update
    return (newest_top, row_total, weighted)


def per_device(
    tokens,
    doc_lengths,
    query_down,
    latent_down,
    rope_down,
    query_latent_gain,
    latent_gain,
    query_up,
    key_up,
    value_up,
    query_gain,
    key_gain,
    output_gain,
    output_weight,
):
    query_latent = norm_rows(
        jnp.dot(tokens, query_down, preferred_element_type=jnp.float32), query_latent_gain
    ).astype(jnp.bfloat16)
    key_latent = norm_rows(
        jnp.dot(tokens, latent_down, preferred_element_type=jnp.float32), latent_gain
    ).astype(jnp.bfloat16)
    rope_key = jnp.dot(tokens, rope_down, preferred_element_type=jnp.float32).astype(jnp.bfloat16)
    query_rows, latent_rows, rope_rows = (
        lax.all_gather(query_latent, "tp", axis=0, tiled=True),
        lax.all_gather(key_latent, "tp", axis=0, tiled=True),
        lax.all_gather(rope_key, "tp", axis=0, tiled=True),
    )
    row_count = query_rows.shape[0]
    head_width = NOPE + ROPE
    head_count = query_up.shape[1] // head_width
    row_offset = lax.axis_index("sp") * row_count
    places = row_offset + jnp.arange(row_count, dtype=jnp.int32)
    doc_ends = jnp.cumsum(doc_lengths)
    query_docs = doc_index(places, doc_ends)
    lowest_doc = query_docs[0]
    highest_doc = query_docs[row_count - 1]
    query_raw = jnp.dot(query_rows, query_up, preferred_element_type=jnp.float32).reshape(
        row_count, head_count, head_width
    )
    query_raw = norm_rows(query_raw, query_gain)
    queries = jnp.concatenate(
        [query_raw[..., :NOPE], rotate(query_raw[..., NOPE:], places)], axis=-1
    ).astype(jnp.bfloat16)
    score_scale = head_width ** (-0.5)
    initial = (
        jnp.full((head_count, row_count), NEG, jnp.float32),
        jnp.zeros((head_count, row_count), jnp.float32),
        jnp.zeros((row_count, head_count, VD), jnp.float32),
    )

    def from_latent(sliced, key_places):
        return head_keys(sliced[0], sliced[1], key_places, key_up, value_up, key_gain)

    pieces = (
        lax.all_gather(latent_rows, "sp", axis=0, tiled=True),
        lax.all_gather(rope_rows, "sp", axis=0, tiled=True),
    )
    piece_rows = pieces[0].shape[0]
    span_rows = math.gcd(piece_rows, key_span)

    def one_span(turn_index, carried):
        offset = turn_index * span_rows
        sliced = tuple(
            (lax.dynamic_slice_in_dim(member, offset, span_rows, 0) for member in pieces)
        )
        key_places = offset + jnp.arange(span_rows, dtype=jnp.int32)
        key_docs = doc_index(key_places, doc_ends)
        touches = (key_docs[0] <= highest_doc) & (key_docs[span_rows - 1] >= lowest_doc)

        def absorb_span(current):
            key_block, value_block = from_latent(sliced, key_places)
            return absorb_block(
                current, queries, query_docs, key_block, value_block, key_docs, score_scale
            )

        def pass_over(current):
            return current

        return lax.cond(touches, absorb_span, pass_over, carried)

    row_top, row_total, weighted = lax.fori_loop(0, piece_rows // span_rows, one_span, initial)
    head_out = (
        (weighted / jnp.transpose(row_total)[:, :, None])
        .astype(jnp.bfloat16)
        .reshape(row_count, head_count * VD)
    )
    log_totals = row_top + jnp.log(row_total)
    every_head = lax.all_gather(head_out, "tp", axis=1, tiled=True)
    normed = norm_rows(every_head.astype(jnp.float32), output_gain).astype(jnp.bfloat16)
    layer_output = jnp.dot(normed, output_weight, preferred_element_type=jnp.float32).astype(
        jnp.bfloat16
    )
    return (layer_output, log_totals)


def solution(mesh):
    return jax.shard_map(
        per_device,
        mesh=mesh,
        in_specs=(
            P(("sp", "tp"), None),
            P(),
            P(),
            P(),
            P(),
            P(),
            P(),
            P(None, "tp"),
            P(None, "tp"),
            P(None, "tp"),
            P(),
            P(),
            P(),
            P(None, "tp"),
        ),
        out_specs=(P("sp", "tp"), P("tp", "sp")),
        check_vma=False,
    )
```

profile of v0, /device:TPU:0, one launch (start us, length us, event | category | flops | bytes accessed | tf_op | source)
XLA Modules:
  0.0 103.3 jit_solution(12043495153674618477)
XLA Ops:
  0.6 0.0 copy-start
  0.6 0.0 copy-start.1
  0.7 0.0 copy-start.9
  0.7 0.0 copy-start.2
  0.7 0.0 copy-start.11
  0.7 0.0 copy-start.12
  0.7 0.0 copy-start.10
  0.7 1.7 %copy-done = bf16[2048,512]{1,0:T(8,128)(2,1)S(1)} copy-done((bf16[2048,512]{1,0:T(8,128)(2,1)S(1)}, bf16[2048,512]{1,0:T(8,128)(2,1)}, u32[]{:S(2)}) %copy-start) | copy-done | bytes 2097176
  2.4 1.5 %multiply_reduce_fusion.2 = (f32[32]{0:T(128)S(1)}, f32[32,512]{1,0:T(8,128)S(1)}) fusion(bf16[32,2048]{1,0:T(8,128)(2,1)} %param.16, bf16[2048,512]{1,0:T(8,128)(2,1)S(1)} %copy-done), kind=kOutput, calls=%fused_computation.49 | convolution fusion | flops 67141600 | bytes 2293888 | tf_op jit(solution)/shard_map/dot_general | solution.py:96
  3.8 0.0 copy-start.3
  3.9 0.0 copy-start.4
  3.9 0.0 copy-done.9
  3.9 0.1 multiply_convert_fusion
  4.0 6.5 %all_gather.22 = bf16[128,512]{1,0:T(8,128)(2,1)S(1)} all-gather(bf16[32,512]{1,0:T(8,128)(2,1)S(1)} %multiply_convert_fusion), channel_id=1, replica_groups=mesh['sp'=8,'tp'=4] {'tp'}, dimensions={0}, use_global_device_ids=true | all-gather | bytes 163840 | tf_op jit(solution)/shard_map/all_gather | solution.py:103
  10.5 0.0 copy-done.2
  10.5 0.2 fusion.28
  10.7 0.0 copy-done.11
  10.7 0.1 multiply_multiply_fusion.1
  10.8 0.1 multiply_cosine_fusion.2
  11.0 0.6 pad_maximum_fusion.1
  11.6 0.0 copy-done.12
  11.6 0.1 copy.29
  11.8 0.1 reduce
  11.9 0.1 convert_reduce_fusion.1
  12.0 0.0 copy-done.1
  12.0 1.6 %multiply_reduce_fusion.3 = (f32[32]{0:T(128)S(1)}, f32[32,256]{1,0:T(8,128)S(1)}) fusion(bf16[32,2048]{1,0:T(8,128)(2,1)S(1)} %copy-done.1, bf16[2048,256]{1,0:T(8,128)(2,1)} %param.19), kind=kOutput, calls=%fused_computation.54 | convolution fusion | flops 33570784 | bytes 1212544 | tf_op jit(solution)/shard_map/dot_general | solution.py:99
  13.6 0.0 copy-done.10
  13.6 0.1 multiply_convert_fusion.1
  13.7 5.4 %all_gather.18 = bf16[128,256]{1,0:T(8,128)(2,1)S(1)} all-gather(bf16[32,256]{1,0:T(8,128)(2,1)S(1)} %multiply_convert_fusion.1), channel_id=1, replica_groups=mesh['sp'=8,'tp'=4] {'tp'}, dimensions={0}, use_global_device_ids=true | all-gather | bytes 81920 | tf_op jit(solution)/shard_map/all_gather | solution.py:104
  19.1 32.1 %all_gather.19 = bf16[1024,256]{1,0:T(8,128)(2,1)S(1)} all-gather(bf16[128,256]{1,0:T(8,128)(2,1)S(1)} %all_gather.18), channel_id=1, replica_groups=mesh['sp'=8,'tp'=4] {'sp'}, dimensions={0}, use_global_device_ids=true | all-gather | bytes 589824 | tf_op jit(solution)/shard_map/all_gather | solution.py:134
  51.2 0.1 convert_reduce_fusion
  51.3 0.0 copy-done.3
  51.3 0.2 convolution_convert_fusion.2
  51.4 5.2 %all_gather.20 = bf16[128,32]{1,0:T(8,128)(2,1)S(1)} all-gather(bf16[32,32]{1,0:T(8,128)(2,1)S(1)} %convolution_convert_fusion.2), channel_id=1, replica_groups=mesh['sp'=8,'tp'=4] {'tp'}, dimensions={0}, use_global_device_ids=true | all-gather | bytes 10240 | tf_op jit(solution)/shard_map/all_gather | solution.py:105
  56.6 30.7 %all_gather.21 = bf16[1024,32]{1,0:T(8,128)(2,1)S(1)} all-gather(bf16[128,32]{1,0:T(8,128)(2,1)S(1)} %all_gather.20), channel_id=1, replica_groups=mesh['sp'=8,'tp'=4] {'sp'}, dimensions={0}, use_global_device_ids=true | all-gather | bytes 73728 | tf_op jit(solution)/shard_map/all_gather | solution.py:135
  87.4 0.6 fusion.25
  90.5 0.0 copy-done.4
  90.5 4.6 %conditional.1 = (f32[2,128]{1,0:T(2,128)S(1)}, f32[128,2,64]{0,2,1:T(8,128)S(1)}, f32[2,128]{1,0:T(2,128)S(1)}) conditional(s32[]{:T(128)} %bitcast.1, (f32[2,128]{1,0:T(2,128)S(1)}, f32[2,128]{1,0:T(2,128)S(1)}, f32[128,2,64]{0,2,1:T(8,128)S(1)}) %tuple.27, (s32[128]{0:T(128)S(1)}, s32[1024]{0:T(1024)S(1)}, ...), branch_computations={%region_6.7_spmd.clone, %region_7.11_spmd.clone} | conditional | flops 223451936 | bytes 11297928 | solution.py:158
  90.6 0.0 copy-start.7
  90.6 0.6 copy-done.7
  91.1 0.3 fusion.27
  91.5 0.1 copy.30
  91.6 0.0 copy-start.8
  91.6 0.0 copy-start.6
  91.6 0.1 multiply_reduce_fusion
  91.7 0.8 multiply_multiply_fusion
  92.5 0.0 copy-start.5
  92.6 0.9 multiply_cosine_fusion.1
  93.6 0.0 copy-done.8
  93.6 0.2 broadcast_compare_fusion
  93.8 0.0 copy-done.6
  93.8 0.4 fusion.24
  94.2 0.0 copy-done.5
  94.2 0.3 convolution_convert_fusion
  94.5 0.4 fusion.2
  94.9 0.2 fusion.4
  95.2 0.6 log_add_fusion
  95.8 5.4 %all_gather.23 = bf16[128,512]{0,1:T(8,128)(2,1)S(1)} all-gather(bf16[128,128]{0,1:T(8,128)(2,1)S(1)} %bitcast.37), channel_id=1, replica_groups=mesh['sp'=8,'tp'=4] {'tp'}, dimensions={1}, use_global_device_ids=true | all-gather | bytes 163840 | tf_op jit(solution)/shard_map/all_gather | solution.py:167
  101.2 0.1 fusion.17
  101.3 2.1 %convolution_convert_fusion.1 = bf16[128,512]{1,0:T(8,128)(2,1)} fusion(bf16[512,512]{1,0:T(8,128)(2,1)} %param.29, bf16[128,512]{0,1:T(8,128)(2,1)S(1)} %all_gather.23, f32[512]{0:T(512)} %param.28, f32[128]{0:T(128)S(1)} %add_rsqrt_fusion.2), kind=kOutput, calls=%fused_computation.35 | convolution fusion | flops 67436544 | bytes 788992 | tf_op jit(solution)/shard_map/dot_general | solution.py:169
  (28 shorter events, 0.3 us)
Async XLA Ops:
  0.6 1.7 %copy-start = (bf16[2048,512]{1,0:T(8,128)(2,1)S(1)}, bf16[2048,512]{1,0:T(8,128)(2,1)}, u32[]{:S(2)}) copy-start(bf16[2048,512]{1,0:T(8,128)(2,1)} %param.18) | copy-start | bytes 6291460
  0.6 11.3 %copy-start.1 = (bf16[32,2048]{1,0:T(8,128)(2,1)S(1)}, bf16[32,2048]{1,0:T(8,128)(2,1)}, u32[]{:S(2)}) copy-start(bf16[32,2048]{1,0:T(8,128)(2,1)} %param.16) | copy-start | bytes 393220
  0.7 3.2 %copy-start.9 = (f32[512]{0:T(512)S(1)}, f32[512]{0:T(512)}, u32[]{:S(2)}) copy-start(f32[512]{0:T(512)} %param.21) | copy-start | bytes 6148
  0.7 9.8 %copy-start.2 = (bf16[512,192]{0,1:T(8,128)(2,1)S(1)}, bf16[512,192]{0,1:T(8,128)(2,1)}, u32[]{:S(2)}) copy-start(bf16[512,192]{0,1:T(8,128)(2,1)} %param.23) | copy-start | bytes 589828
  0.7 10.1 %copy-start.11 = (f32[96]{0:T(128)S(1)}, f32[96]{0:T(128)}, u32[]{:S(2)}) copy-start(f32[96]{0:T(128)} %param.26) | copy-start | bytes 1156
  0.7 10.9 %copy-start.12 = (s32[16]{0:T(128)S(1)}, s32[16]{0:T(128)}, u32[]{:S(2)}) copy-start(s32[16]{0:T(128)} %param.17) | copy-start | bytes 196
  0.7 12.9 %copy-start.10 = (f32[256]{0:T(256)S(1)}, f32[256]{0:T(256)}, u32[]{:S(2)}) copy-start(f32[256]{0:T(256)} %param.22) | copy-start | bytes 3076
  3.8 47.4 %copy-start.3 = (bf16[2048,32]{0,1:T(8,128)(2,1)S(1)}, bf16[2048,32]{0,1:T(8,128)(2,1)}, u32[]{:S(2)}) copy-start(bf16[2048,32]{0,1:T(8,128)(2,1)} %param.20) | copy-start | bytes 393220
  3.9 86.7 %copy-start.4 = (bf16[256,128]{1,0:T(8,128)(2,1)S(1)}, bf16[256,128]{1,0:T(8,128)(2,1)}, u32[]{:S(2)}) copy-start(bf16[256,128]{1,0:T(8,128)(2,1)} %param.24) | copy-start | bytes 196612
  90.6 0.6 copy-start.7
  91.6 2.0 %copy-start.8 = (s32[128]{0:T(128)S(1)}, s32[128]{0:T(128)}, u32[]{:S(2)}) copy-start(s32[128]{0:T(128)} %copy-done.7) | copy-start | bytes 1540 | tf_op jit(solution)/shard_map/while/body/eval_jaxpr/cond
  91.6 2.2 %copy-start.6 = (bf16[128,2,96]{0,2,1:T(8,128)(2,1)S(1)}, bf16[128,2,96]{0,2,1:T(8,128)(2,1)}, u32[]{:S(2)}) copy-start(bf16[128,2,96]{0,2,1:T(8,128)(2,1)} %get-tuple-element.141) | copy-start | bytes 147460 | tf_op jit(solution)/shard_map/while/body/eval_jaxpr/cond
  92.5 1.7 %copy-start.5 = (bf16[256,128]{1,0:T(8,128)(2,1)S(1)}, bf16[256,128]{1,0:T(8,128)(2,1)}, u32[]{:S(2)}) copy-start(bf16[256,128]{1,0:T(8,128)(2,1)} %get-tuple-element.146) | copy-start | bytes 196612 | tf_op jit(solution)/shard_map/while/body/eval_jaxpr/cond
where the time goes:
time: 104 us; the launch traced here: 103 us
  blocking collectives  85.3 us (82%)
  matrix products  6.87 us (7%)
  other arithmetic  4.36 us (4%)
  between operations  3.4 us (3%)
  local copies, waits for them, and re-layouts  3.18 us (3%)
    all_gather x1, blocking collectives, per_device(): lax.all_gather(latent_rows, 'sp', axis=0, tiled=True)  32.1 us
    all_gather x1, blocking collectives, per_device(): lax.all_gather(rope_rows, 'sp', axis=0, tiled=True)  30.7 us
    all_gather x1, blocking collectives, per_device(): lax.all_gather(query_latent, 'tp', axis=0, tiled=True)  6.49 us
    all_gather x1, blocking collectives, per_device(): every_head = lax.all_gather(head_out, 'tp', axis=1, tiled=True)  5.42 us
    all_gather x1, blocking collectives, per_device(): lax.all_gather(key_latent, 'tp', axis=0, tiled=True)  5.39 us
    all_gather x1, blocking collectives, per_device(): lax.all_gather(rope_key, 'tp', axis=0, tiled=True)  5.19 us

commit v1 on v0

--- a/solution.py
+++ b/solution.py
@@ -11,6 +11,11 @@
 THETA = 10000.0
 NEG = -1e30
 key_span = 2048
+
+
+def all_by_exchange(array, name, dim):
+    outgoing = jnp.stack([array] * lax.axis_size(name))
+    return jnp.concatenate(lax.all_to_all(outgoing, name, 0, 0), axis=dim)
 
 
 def norm_rows(matrix, scaling):
@@ -132,7 +137,7 @@
 
     pieces = (
         lax.all_gather(latent_rows, "sp", axis=0, tiled=True),
-        lax.all_gather(rope_rows, "sp", axis=0, tiled=True),
+        all_by_exchange(rope_rows, "sp", 0),
     )
     piece_rows = pieces[0].shape[0]
     span_rows = math.gcd(piece_rows, key_span)

time: 104 us -> 75 us (0.72)
  blocking collectives: 85.3 us -> 54.3 us
  starting transfers between devices: 0 us -> 6.3 us
  local copies, waits for them, and re-layouts: 3.18 us -> 1.59 us
  other arithmetic: 4.36 us -> 3.14 us
  matrix products: 6.87 us -> 5.74 us
    all_gather x1 -> x0, blocking collectives: 30.7 us -> none  [per_device(): lax.all_gather(rope_rows, 'sp', axis=0, tiled=True)]
    all_to_all x0 -> x1, starting transfers between devices: none -> 6.3 us  [all_by_exchange(): return jnp.concatenate(lax.all_to_all(outgoing, name, 0, 0), axis=dim)]
    unnamed x18 -> x24, local copies, waits for them, and re-layouts: 1.71 us -> 0.07 us
    dot_general x1, matrix products: 1.62 us -> 0.39 us  [per_device(): jnp.dot(tokens, latent_down, preferred_element_type=jnp.float32)]
    dot_general x1, matrix products: 0.16 us -> 1.27 us  [per_device(): jnp.dot(tokens, rope_down, preferred_element_type=jnp.float32)]
    all_gather x1, blocking collectives: 6.49 us -> 5.4 us  [per_device(): lax.all_gather(query_latent, 'tp', axis=0, tiled=True)]
    dot_general x1, matrix products: 2.06 us -> 1 us  [per_device(): jnp.dot(normed, output_weight, preferred_element_type=jnp.float32)]
  transfers between devices with their start and end apart: 0 -> 1, of which waited for: 0 -> 0; matrix products, arithmetic and copies ran while one was open for 0% -> 5% of each run, Pallas kernels for 0% -> 0%
where the time goes in v1:
time: 75 us; the launch traced here: 74.7 us
  blocking collectives  54.3 us (72%)
  starting transfers between devices  6.3 us (8%)
  matrix products  5.74 us (8%)
  between operations  3.47 us (5%)
  other arithmetic  3.14 us (4%)
  local copies, waits for them, and re-layouts  1.59 us (2%)
    all_gather x1, blocking collectives, per_device(): lax.all_gather(latent_rows, 'sp', axis=0, tiled=True)  32 us
    all_to_all x1, starting transfers between devices, all_by_exchange(): return jnp.concatenate(lax.all_to_all(outgoing, name, 0, 0), axis=dim)  6.3 us
    all_gather x1, blocking collectives, per_device(): lax.all_gather(rope_key, 'tp', axis=0, tiled=True)  6.21 us
    all_gather x1, blocking collectives, per_device(): every_head = lax.all_gather(head_out, 'tp', axis=1, tiled=True)  5.42 us
    all_gather x1, blocking collectives, per_device(): lax.all_gather(query_latent, 'tp', axis=0, tiled=True)  5.4 us
    all_gather x1, blocking collectives, per_device(): lax.all_gather(key_latent, 'tp', axis=0, tiled=True)  5.22 us
    dot_general x1, matrix products, per_device(): jnp.dot(tokens, query_down, preferred_element_type=jnp.float32)  1.5 us
  transfers between devices with their start and end apart: 1, of which 0 were waited for; matrix products, arithmetic and copies ran while one was open for 5% of the time, Pallas kernels for 0%

profile of v1, /device:TPU:0, one launch (start us, length us, event | category | flops | bytes accessed | tf_op | source)
XLA Modules:
  0.0 74.7 jit_solution(6458029382664529090)
XLA Ops:
  0.6 0.0 copy-start
  0.6 0.0 copy-start.1
  0.7 0.0 copy-start.8
  0.7 0.0 copy-start.12
  0.7 0.0 copy-start.2
  0.7 1.3 %convolution_convert_fusion.2 = bf16[32,32]{1,0:T(8,128)(2,1)S(1)} fusion(bf16[32,2048]{1,0:T(8,128)(2,1)} %param.16, bf16[2048,32]{0,1:T(8,128)(2,1)} %param.20), kind=kOutput, calls=%fused_computation.38 | convolution fusion | flops 4195328 | bytes 264192 | tf_op jit(solution)/shard_map/dot_general | solution.py:106
  2.0 6.2 %all_gather.17 = bf16[128,32]{1,0:T(8,128)(2,1)S(1)} all-gather(bf16[32,32]{1,0:T(8,128)(2,1)S(1)} %convolution_convert_fusion.2), channel_id=1, replica_groups=mesh['sp'=8,'tp'=4] {'tp'}, dimensions={0}, use_global_device_ids=true | all-gather | bytes 10240 | tf_op jit(solution)/shard_map/all_gather | solution.py:110
  8.2 0.1 copy.34
  8.2 0.7 stack.2
  8.9 6.3 %all-to-all-start = ((bf16[8,128,32]{1,2,0:T(8,128)(2,1)}), bf16[8,128,32]{1,2,0:T(8,128)(2,1)S(1)}, u32[]{:S(2)}, u32[]{:S(2)}) async-start(bf16[8,128,32]{1,2,0:T(8,128)(2,1)} %stack.2), calls=%async_computation | async-start | bytes 131072 | tf_op jit(solution)/shard_map/all_to_all | solution.py:18
  15.2 0.0 copy-start.4
  15.2 0.0 copy-done
  15.3 0.0 copy-start.9
  15.3 0.0 copy-start.10
  15.3 1.5 %multiply_reduce_fusion.2 = (f32[32]{0:T(128)S(1)}, f32[32,512]{1,0:T(8,128)S(1)}) fusion(bf16[32,2048]{1,0:T(8,128)(2,1)} %param.16, bf16[2048,512]{1,0:T(8,128)(2,1)S(1)} %copy-done), kind=kOutput, calls=%fused_computation.51 | convolution fusion | flops 67141600 | bytes 2293888 | tf_op jit(solution)/shard_map/dot_general | solution.py:101
  16.8 0.0 copy-start.5
  16.8 0.0 copy-start.11
  16.8 0.0 copy-done.8
  16.8 0.1 multiply_convert_fusion
  16.9 5.4 %all_gather.18 = bf16[128,512]{1,0:T(8,128)(2,1)S(1)} all-gather(bf16[32,512]{1,0:T(8,128)(2,1)S(1)} %multiply_convert_fusion), channel_id=1, replica_groups=mesh['sp'=8,'tp'=4] {'tp'}, dimensions={0}, use_global_device_ids=true | all-gather | bytes 163840 | tf_op jit(solution)/shard_map/all_gather | solution.py:108
  22.3 0.0 copy-done.4
  22.3 0.2 fusion.28
  22.6 0.0 copy-done.12
  22.6 0.1 copy.33
  22.7 0.1 reduce
  22.8 0.1 convert_reduce_fusion
  22.9 0.1 convert_reduce_fusion.1
  23.0 0.0 copy-done.1
  23.0 0.0 copy-done.2
  23.0 0.4 multiply_reduce_fusion.3
  23.4 0.0 copy-done.9
  23.4 0.1 multiply_convert_fusion.1
  23.5 5.2 %all_gather.15 = bf16[128,256]{1,0:T(8,128)(2,1)S(1)} all-gather(bf16[32,256]{1,0:T(8,128)(2,1)S(1)} %multiply_convert_fusion.1), channel_id=1, replica_groups=mesh['sp'=8,'tp'=4] {'tp'}, dimensions={0}, use_global_device_ids=true | all-gather | bytes 81920 | tf_op jit(solution)/shard_map/all_gather | solution.py:109
  28.7 32.0 %all_gather.16 = bf16[1024,256]{1,0:T(8,128)(2,1)S(1)} all-gather(bf16[128,256]{1,0:T(8,128)(2,1)S(1)} %all_gather.15), channel_id=1, replica_groups=mesh['sp'=8,'tp'=4] {'sp'}, dimensions={0}, use_global_device_ids=true | all-gather | bytes 589824 | tf_op jit(solution)/shard_map/all_gather | solution.py:139
  60.8 0.0 copy-done.10
  60.8 0.1 multiply_multiply_fusion.1
  60.9 0.1 multiply_cosine_fusion.2
  61.0 0.6 fusion.25
  64.2 0.0 all-to-all-done
  64.2 0.0 copy-done.5
  64.2 0.0 copy-done.11
  64.2 0.0 copy-start.3
  64.2 0.0 copy-start.7
  64.2 3.3 %conditional.1 = (f32[2,128]{1,0:T(2,128)S(1)}, f32[128,2,64]{0,2,1:T(8,128)S(1)}, f32[2,128]{1,0:T(2,128)S(1)}) conditional(s32[]{:T(128)} %bitcast.1, (f32[2,128]{1,0:T(2,128)S(1)}, f32[2,128]{1,0:T(2,128)S(1)}, f32[128,2,64]{0,2,1:T(8,128)S(1)}) %tuple.27, (s32[128]{0:T(128)S(1)}, s32[1024]{0:T(1024)S(1)}, ...), branch_computations={%region_6.7_spmd.clone, %region_7.11_spmd.clone} | conditional | flops 223484704 | bytes 11490356 | solution.py:163
  64.3 0.3 fusion.27
  64.7 0.1 multiply_reduce_fusion
  64.8 0.1 multiply_multiply_fusion
  64.9 0.0 copy-start.6
  65.0 0.9 %multiply_cosine_fusion.1 = (f32[1024,16]{0,1:T(8,128)S(1)}, f32[1024,16]{0,1:T(8,128)S(1)}, f32[1024,16]{0,1:T(8,128)S(1)}, f32[1024,16]{0,1:T(8,128)S(1)}) fusion(f32[16]{0:T(128)S(1)} %multiply_power_fusion, f32[1024]{0:T(1024)S(1)} %convert_element_type.79, f32[1024]{0:T(1024)S(1)} %convert_element_type.80, f32[1024]{0:T(1024)S(1)} %convert_element_type.81, ...), kind=kLoop, calls=%fused_computation.29 | loop fusion | flops 65536 | bytes 278592 | tf_op jit(solution)/shard_map/while/body/eval_jaxpr/cond/branch_1_fun/cos | solution.py:30
  66.0 0.2 broadcast_compare_fusion
  66.2 0.4 fusion.24
  66.6 0.0 copy-done.6
  66.6 0.3 convolution_convert_fusion
  66.9 0.4 fusion.2
  67.3 0.2 fusion.4
  67.6 0.6 log_add_fusion
  68.2 5.4 %all_gather.19 = bf16[128,512]{0,1:T(8,128)(2,1)S(1)} all-gather(bf16[128,128]{0,1:T(8,128)(2,1)S(1)} %bitcast.45), channel_id=1, replica_groups=mesh['sp'=8,'tp'=4] {'tp'}, dimensions={1}, use_global_device_ids=true | all-gather | bytes 163840 | tf_op jit(solution)/shard_map/all_gather | solution.py:172
  73.6 0.1 fusion.17
  73.7 0.0 copy-done.3
  73.7 0.0 copy-done.7
  73.7 1.0 %convolution_convert_fusion.1 = bf16[128,512]{1,0:T(8,128)(2,1)} fusion(bf16[512,512]{1,0:T(8,128)(2,1)S(1)} %copy-done.3, bf16[128,512]{0,1:T(8,128)(2,1)S(1)} %all_gather.19, f32[512]{0:T(512)S(1)} %copy-done.7, f32[128]{0:T(128)S(1)} %add_rsqrt_fusion.2), kind=kOutput, calls=%fused_computation.37 | convolution fusion | flops 67436544 | bytes 788992 | tf_op jit(solution)/shard_map/dot_general | solution.py:174
  (31 shorter events, 0.4 us)
Async XLA Ops:
  0.6 14.6 %copy-start = (bf16[2048,512]{1,0:T(8,128)(2,1)S(1)}, bf16[2048,512]{1,0:T(8,128)(2,1)}, u32[]{:S(2)}) copy-start(bf16[2048,512]{1,0:T(8,128)(2,1)} %param.18) | copy-start | bytes 6291460
  0.6 22.4 %copy-start.1 = (bf16[32,2048]{1,0:T(8,128)(2,1)S(1)}, bf16[32,2048]{1,0:T(8,128)(2,1)}, u32[]{:S(2)}) copy-start(bf16[32,2048]{1,0:T(8,128)(2,1)} %param.16) | copy-start | bytes 393220
  0.7 16.2 %copy-start.8 = (f32[512]{0:T(512)S(1)}, f32[512]{0:T(512)}, u32[]{:S(2)}) copy-start(f32[512]{0:T(512)} %param.21) | copy-start | bytes 6148
  0.7 21.9 %copy-start.12 = (s32[16]{0:T(128)S(1)}, s32[16]{0:T(128)}, u32[]{:S(2)}) copy-start(s32[16]{0:T(128)} %param.17) | copy-start | bytes 196
  0.7 22.3 %copy-start.2 = (bf16[2048,256]{1,0:T(8,128)(2,1)S(1)}, bf16[2048,256]{1,0:T(8,128)(2,1)}, u32[]{:S(2)}) copy-start(bf16[2048,256]{1,0:T(8,128)(2,1)} %param.19) | copy-start | bytes 3145732
  8.9 55.3 %all-to-all-start = ((bf16[8,128,32]{1,2,0:T(8,128)(2,1)}), bf16[8,128,32]{1,2,0:T(8,128)(2,1)S(1)}, u32[]{:S(2)}, u32[]{:S(2)}) async-start(bf16[8,128,32]{1,2,0:T(8,128)(2,1)} %stack.2), calls=%async_computation | async-start | bytes 131072 | tf_op jit(solution)/shard_map/all_to_all | solution.py:18
  15.2 7.1 %copy-start.4 = (bf16[512,192]{0,1:T(8,128)(2,1)S(1)}, bf16[512,192]{0,1:T(8,128)(2,1)}, u32[]{:S(2)}) copy-start(bf16[512,192]{0,1:T(8,128)(2,1)} %param.23) | copy-start | bytes 589828
  15.3 8.2 %copy-start.9 = (f32[256]{0:T(256)S(1)}, f32[256]{0:T(256)}, u32[]{:S(2)}) copy-start(f32[256]{0:T(256)} %param.22) | copy-start | bytes 3076
  15.3 45.5 %copy-start.10 = (f32[96]{0:T(128)S(1)}, f32[96]{0:T(128)}, u32[]{:S(2)}) copy-start(f32[96]{0:T(128)} %param.26) | copy-start | bytes 1156
  16.8 47.4 %copy-start.5 = (bf16[256,128]{1,0:T(8,128)(2,1)S(1)}, bf16[256,128]{1,0:T(8,128)(2,1)}, u32[]{:S(2)}) copy-start(bf16[256,128]{1,0:T(8,128)(2,1)} %param.24) | copy-start | bytes 196612
  16.8 47.4 %copy-start.11 = (f32[96]{0:T(128)S(1)}, f32[96]{0:T(128)}, u32[]{:S(2)}) copy-start(f32[96]{0:T(128)} %param.27) | copy-start | bytes 1156
  64.2 9.4 %copy-start.3 = (bf16[512,512]{1,0:T(8,128)(2,1)S(1)}, bf16[512,512]{1,0:T(8,128)(2,1)}, u32[]{:S(2)}) copy-start(bf16[512,512]{1,0:T(8,128)(2,1)} %param.29) | copy-start | bytes 1572868
  64.2 9.4 %copy-start.7 = (f32[512]{0:T(512)S(1)}, f32[512]{0:T(512)}, u32[]{:S(2)}) copy-start(f32[512]{0:T(512)} %param.28) | copy-start | bytes 6148
  64.9 1.7 %copy-start.6 = (bf16[256,128]{1,0:T(8,128)(2,1)S(1)}, bf16[256,128]{1,0:T(8,128)(2,1)}, u32[]{:S(2)}) copy-start(bf16[256,128]{1,0:T(8,128)(2,1)} %get-tuple-element.147) | copy-start | bytes 196612 | tf_op jit(solution)/shard_map/while/body/eval_jaxpr/cond
